TPU v7x, 256 devices: a 4x2x16 block of a 4x16x16 slice. The times are simulated.
256 devices in a mesh: grp: 2 (over y), ep: 64 (over z, x), tp: 2 (over core).
Axes of the slice: x: 4, y: 2, z: 16, core: 2. Of those that a mesh axis runs over, the one named last changes fastest.
The devices are a block of a 4x16x16 slice.
Arguments:
- tokens: bfloat16 [4096, 1024], P(('grp', 'ep', 'tp')), parts along dimension 0, may hold values from -1.75 to 1.75
- latent_cache: bfloat16 [4096, 1024, 256], P(('grp', 'ep', 'tp')), parts along dimension 0, may hold values from -6 to 6
- rope_cache: bfloat16 [4096, 1024, 32], P(('grp', 'ep', 'tp')), parts along dimension 0, may hold values from -1200 to 1200
- lengths: int32 [4096], P(('grp', 'ep', 'tp')), parts along dimension 0, may hold values from 128 to 1024
- expert_ids: int32 [4096, 4], P(('grp', 'ep', 'tp')), parts along dimension 0, may hold values from 0 to 127, all different within a row; in each aligned block of 16 rows (0 to 15, 16 to 31, ...) at most 4 rows name the same one
- route_weights: float32 [4096, 4], P(('grp', 'ep', 'tp')), parts along dimension 0, may hold values from 0.1 to 1
- g_attn: float32 [1024], replicated, may hold values from 0.1 to 1.9
- w_query_down: bfloat16 [1024, 256], replicated, may hold values from -0.1875 to 0.1875
- g_query: float32 [256], replicated, may hold values from 0.1 to 1.9
- w_latent_down: bfloat16 [1024, 256], replicated, may hold values from -0.1875 to 0.1875
- g_latent: float32 [256], replicated, may hold values from 0.1 to 1.9
- w_rope_key: bfloat16 [1024, 32], replicated, may hold values from -0.1875 to 0.1875
- w_query: bfloat16 [256, 1024], replicated, may hold values from -0.375 to 0.375
- w_query_rope: bfloat16 [256, 512], replicated, may hold values from -0.375 to 0.375
- w_key_up: bfloat16 [256, 1024], replicated, may hold values from -0.875 to 0.875
- w_value_up: bfloat16 [256, 1024], replicated, may hold values from -0.375 to 0.375
- w_out: bfloat16 [1024, 1024], replicated, may hold values from -0.1875 to 0.1875
- g_ffn: float32 [1024], replicated, may hold values from 0.1 to 1.9
- w_expert_gate: bfloat16 [128, 1024, 256], P('ep', None, 'tp'), may hold values from -0.1875 to 0.1875
- w_expert_up: bfloat16 [128, 1024, 256], P('ep', None, 'tp'), may hold values from -0.1875 to 0.1875
- w_expert_down: bfloat16 [128, 256, 1024], P('ep', 'tp'), may hold values from -0.375 to 0.375
- w_shared_gate: bfloat16 [1024, 256], replicated, may hold values from -0.1875 to 0.1875
- w_shared_up: bfloat16 [1024, 256], replicated, may hold values from -0.1875 to 0.1875
- w_shared_down: bfloat16 [256, 1024], replicated, may hold values from -0.375 to 0.375
Outputs:
- mixed_out: bfloat16 [4096, 1024], P(('grp', 'ep', 'tp')), parts along dimension 0
- new_entry: bfloat16 [4096, 288], P(('grp', 'ep', 'tp')), parts along dimension 0
There are 2 independent parts, one for each index of `grp`. A program takes and returns all parts, laid end to end along the dimension named above; an argument that names none is the same for every part. Nothing has to cross between parts.
Inputs may be any that keep to these rules, and one draw needn't show every extreme that they name: `expert_ids`: each row names 4 different experts. In the aligned blocks of rows that one device holds (one block for each device of ep and tp together), no expert is named by more than 4 rows, a bound that some block reaches.
All inputs are finite; a program needn't handle non-finite values.
Results may differ from a plain program's by a relative error of at most 0.03.
Values may be sent and summed in bfloat16 or wider, within the bound.
A program may use at most 64 MiB of HBM per device.

v0:
```python
import jax
import jax.numpy as jnp
from jax import lax
from jax.sharding import PartitionSpec as P

D = 1024
HEADS = 16
KVLORA = 256
NOPE = 64
ROPE = 32
VDIM = 64
CAP = 4


norm_eps = 1e-06
rope_theta = 10000.0
masked_score = -1e30


def copy_for_each(value, axis):
    count = lax.axis_size(axis)
    return lax.all_to_all(
        jnp.broadcast_to(value[None], (count, *value.shape)), axis, 0, 0, tiled=True
    )


def joined_along(blocks, dim):
    blocks = jnp.moveaxis(blocks, 0, dim)
    dims = blocks.shape
    return blocks.reshape(*dims[:dim], dims[dim] * dims[dim + 1], *dims[dim + 2 :])


def gathered_copies(value, axis, dim):
    blocks = copy_for_each(value, axis)
    return joined_along(blocks, dim)


def split_up(value, dim, count):
    before, after = (value.shape[:dim], value.shape[dim + 1 :])
    return jnp.moveaxis(value.reshape(*before, count, -1, *after), dim, 0)


def sent_and_summed(value, axis, dim):
    count = lax.axis_size(axis)
    blocks = lax.all_to_all(split_up(value, dim, count), axis, 0, 0, tiled=True)
    return jnp.sum(blocks.astype(jnp.float32), axis=0)


def rms_scale(values, gain_vec):
    mean_square = jnp.mean(values * values, axis=-1, keepdims=True)
    return values * lax.rsqrt(mean_square + norm_eps) * gain_vec


def rotate(values, positions):
    half_width = values.shape[-1] // 2
    frequency = rope_theta ** (-jnp.arange(half_width, dtype=jnp.float32) / half_width)
    angles = positions.astype(jnp.float32)[:, None] * frequency[None, :]
    angles = angles.reshape(angles.shape[:1] + (1,) * (values.ndim - 2) + (half_width,))
    cosine = jnp.cos(angles)
    sine_part = jnp.sin(angles)
    first_half = values[..., :half_width]
    second_half = values[..., half_width:]
    return jnp.concatenate(
        [
            first_half * cosine - second_half * sine_part,
            first_half * sine_part + second_half * cosine,
        ],
        axis=-1,
    )


def slot_numbers(expert_ids, expert_count):
    flat_ids = expert_ids.reshape(-1)
    onehot = (flat_ids[:, None] == jnp.arange(expert_count, dtype=jnp.int32)[None, :]).astype(
        jnp.int32
    )
    rank_before = jnp.cumsum(onehot, axis=0) - onehot
    return jnp.sum(rank_before * onehot, axis=1).reshape(expert_ids.shape)


def local(
    tokens,
    latent_cache,
    rope_cache,
    lengths,
    expert_ids,
    route_weights,
    g_attn,
    w_query_down,
    g_query,
    w_latent_down,
    g_latent,
    w_rope_key,
    w_query,
    w_query_rope,
    w_key_up,
    w_value_up,
    w_out,
    g_ffn,
    w_expert_gate,
    w_expert_up,
    w_expert_down,
    w_shared_gate,
    w_shared_up,
    w_shared_down,
):
    row_count = tokens.shape[0]
    normed = rms_scale(tokens.astype(jnp.float32), g_attn).astype(jnp.bfloat16)
    query_low = rms_scale(
        jnp.dot(normed, w_query_down, preferred_element_type=jnp.float32), g_query
    ).astype(jnp.bfloat16)
    latent_new = rms_scale(
        jnp.dot(normed, w_latent_down, preferred_element_type=jnp.float32), g_latent
    ).astype(jnp.bfloat16)
    key_new = rotate(
        jnp.dot(normed, w_rope_key, preferred_element_type=jnp.float32), lengths
    ).astype(jnp.bfloat16)
    new_entry = jnp.concatenate([latent_new, key_new], axis=1)
    query_nope = jnp.dot(query_low, w_query, preferred_element_type=jnp.float32).astype(
        jnp.bfloat16
    )
    query_nope = query_nope.reshape(row_count, HEADS, NOPE)
    query_turn = jnp.dot(query_low, w_query_rope, preferred_element_type=jnp.float32).reshape(
        row_count, HEADS, ROPE
    )
    query_rope = rotate(query_turn, lengths).astype(jnp.bfloat16)
    query_latent = jnp.einsum(
        "bhn,chn->bhc",
        query_nope,
        w_key_up.reshape(KVLORA, HEADS, NOPE),
        preferred_element_type=jnp.float32,
    ).astype(jnp.bfloat16)
    scores = (
        jnp.einsum("shc,stc->sht", query_latent, latent_cache, preferred_element_type=jnp.float32)
        + jnp.einsum("shr,str->sht", query_rope, rope_cache, preferred_element_type=jnp.float32)
    ) * (NOPE + ROPE) ** (-0.5)
    live_mask = (
        jnp.arange(latent_cache.shape[1], dtype=jnp.int32)[None, None, :] < lengths[:, None, None]
    )
    row_max = jnp.max(jnp.where(live_mask, scores, masked_score), axis=2, keepdims=True)
    weights = jnp.where(live_mask, jnp.exp(scores - row_max), 0.0)
    weight_sum = jnp.sum(weights, axis=2)
    mixed_latent = jnp.einsum(
        "sht,stc->shc",
        weights.astype(jnp.bfloat16),
        latent_cache,
        preferred_element_type=jnp.float32,
    )
    latent_mix = (mixed_latent / weight_sum[:, :, None]).astype(jnp.bfloat16)
    value_heads = jnp.einsum(
        "shc,chv->shv",
        latent_mix,
        w_value_up.reshape(KVLORA, HEADS, VDIM),
        preferred_element_type=jnp.float32,
    ).astype(jnp.bfloat16)
    attn_out = jnp.dot(
        value_heads.reshape(row_count, HEADS * VDIM), w_out, preferred_element_type=jnp.float32
    )
    hidden_state = (tokens.astype(jnp.float32) + attn_out).astype(jnp.bfloat16)
    normed_ffn = rms_scale(hidden_state.astype(jnp.float32), g_ffn).astype(jnp.bfloat16)
    shared_gate = jnp.dot(normed_ffn, w_shared_gate, preferred_element_type=jnp.float32)
    shared_up = jnp.dot(normed_ffn, w_shared_up, preferred_element_type=jnp.float32)
    shared_hidden = (jax.nn.silu(shared_gate) * shared_up).astype(jnp.bfloat16)
    shared_out = jnp.dot(shared_hidden, w_shared_down, preferred_element_type=jnp.float32)
    ep_size = lax.axis_size("ep")
    local_experts = w_expert_gate.shape[0]
    expert_count = local_experts * ep_size
    slot_count = expert_count * CAP
    slots = slot_numbers(expert_ids, expert_count)
    target = expert_ids * CAP + slots
    slot_match = target[:, :, None] == jnp.arange(slot_count, dtype=jnp.int32)[None, None, :]
    spread = jnp.sum(slot_match.astype(jnp.bfloat16), axis=1)
    outbox = jnp.einsum("sn,sd->nd", spread, normed_ffn, preferred_element_type=jnp.float32)
    outbox = outbox.astype(jnp.bfloat16).reshape(ep_size, local_experts, CAP, D)
    landed = lax.all_to_all(outbox, "ep", split_axis=0, concat_axis=0, tiled=True)
    arrived = gathered_copies(landed[:, None], "tp", 1)
    gate_value = jnp.einsum(
        "aterd,edf->aterf", arrived, w_expert_gate, preferred_element_type=jnp.float32
    )
    up_value = jnp.einsum(
        "aterd,edf->aterf", arrived, w_expert_up, preferred_element_type=jnp.float32
    )
    hidden = (jax.nn.silu(gate_value) * up_value).astype(jnp.bfloat16)
    partial_value = jnp.einsum(
        "aterf,efd->aterd", hidden, w_expert_down, preferred_element_type=jnp.float32
    )
    summed = sent_and_summed(partial_value.astype(jnp.bfloat16), "tp", 1)
    returned = lax.all_to_all(
        summed[:, 0].astype(jnp.bfloat16), "ep", split_axis=0, concat_axis=0, tiled=True
    )
    slot_weights = jnp.sum(jnp.where(slot_match, route_weights[:, :, None], 0.0), axis=1)
    routed = jnp.dot(slot_weights, returned.reshape(slot_count, D).astype(jnp.float32))
    mixed_out = (hidden_state.astype(jnp.float32) + routed + shared_out).astype(jnp.bfloat16)
    return (mixed_out, new_entry)


def solution(mesh):
    in_specs = (
        P(("grp", "ep", "tp"), None),
        P(("grp", "ep", "tp"), None, None),
        P(("grp", "ep", "tp"), None, None),
        P(("grp", "ep", "tp")),
        P(("grp", "ep", "tp"), None),
        P(("grp", "ep", "tp"), None),
        P(),
        P(),
        P(),
        P(),
        P(),
        P(),
        P(),
        P(),
        P(),
        P(),
        P(),
        P(),
        P("ep", None, "tp"),
        P("ep", None, "tp"),
        P("ep", "tp", None),
        P(),
        P(),
        P(),
    )
    out_specs = (P(("grp", "ep", "tp"), None), P(("grp", "ep", "tp"), None))
    return jax.shard_map(local, mesh=mesh, in_specs=in_specs, out_specs=out_specs, check_vma=False)
```

profile of v0, /device:TPU:40, one launch (start us, length us, event | category | flops | bytes accessed | tf_op | source)
XLA Modules:
  0.0 199.7 jit_solution(12549387200572937520)
XLA Ops:
  3.1 1.4 multiply_reduce_fusion.2
  4.5 1.2 fusion.83
  6.9 1.3 convolution_convert_fusion.3
  8.9 1.6 fusion.59
  10.5 5.7 %fusion.15 = f32[16,16,1024]{2,1,0:T(8,128)S(1)} fusion(f32[16,16,1024]{2,1,0:T(8,128)S(1)} %fusion.59, bf16[16,1024,256]{2,1,0:T(8,128)(2,1)} %param.25, bf16[16,16,256]{2,0,1:T(8,128)(2,1)S(1)} %fusion.29), kind=kOutput, calls=%fused_computation.15 | convolution fusion | flops 134742016 | bytes 10616832 | tf_op jit(solution)/shard_map/shc,stc->sht/dot_general | solution.py:134
  16.6 4.7 %fusion.28 = bf16[16,16,256]{2,1,0:T(8,128)(2,1)S(1)} fusion(bf16[16,1024,256]{2,1,0:T(8,128)(2,1)} %param.25, f32[16,16]{1,0:T(8,128)S(1)} %fusion.90, f32[16,16,1024]{2,1,0:T(8,128)S(1)} %fusion.15, pred[16,1024]{1,0:T(8,128)(4,1)S(1)} %iota_compare_fusion.1), kind=kOutput, calls=%fused_computation.22 | convolution fusion | flops 135398656 | bytes 9585664 | tf_op jit(solution)/shard_map/sht,stc->shc/dot_general | solution.py:143
  21.4 1.3 copy.96
  24.9 1.2 reshape.161
  26.2 82.9 %all_to_all.20 = bf16[64,2,4,1024]{3,2,1,0:T(4,128)(2,1)S(1)} all-to-all(bf16[64,2,4,1024]{3,2,1,0:T(4,128)(2,1)} %reshape.161), channel_id=1, replica_groups=mesh['grp'=2,'ep'=64,'tp'=2] {'ep'}, dimensions={0} | all-to-all | bytes 2097152 | tf_op jit(solution)/shard_map/all_to_all | solution.py:175
  110.0 5.6 %all_to_all.21 = bf16[2,64,1,2,4,1024]{5,1,4,3,2,0:T(8,128)(2,1)S(1)} all-to-all(bf16[2,64,1,2,4,1024]{5,1,4,3,2,0:T(8,128)(2,1)S(1)} %broadcast_in_dim.33), channel_id=1, replica_groups=mesh['grp'=2,'ep'=64,'tp'=2] {'tp'}, dimensions={0} | all-to-all | bytes 4194304 | tf_op jit(solution)/shard_map/all_to_all | solution.py:22
  115.5 1.3 copy-done.1
  116.9 1.5 fusion.16
  118.4 4.2 %convert_bitcast_fusion = bf16[2,64,1,2,4,1024]{5,1,4,0,3,2:T(8,128)(2,1)} fusion(bf16[2,64,1,2,4,1024]{5,1,4,3,2,0:T(8,128)(2,1)} %copy-done.1, bf16[2,128,1024]{2,1,0:T(8,128)(2,1)S(1)} %copy-done.10, bf16[2,1024,128]{2,1,0:T(8,128)(2,1)S(1)} %copy-done.11, f32[64,2,2,4,128]{4,0,3,1,2:T(8,128)} %fusion.16), kind=kOutput, calls=%fused_computation.5 | convolution fusion | flops 538705920 | bytes 5767168 | tf_op jit(solution)/shard_map/aterf,efd->aterd/dot_general | solution.py:184
  122.6 1.8 copy.103
  124.4 6.3 %all_to_all.22 = bf16[2,64,1,2,4,1024]{5,1,4,3,2,0:T(8,128)(2,1)} all-to-all(bf16[2,64,1,2,4,1024]{5,1,4,3,2,0:T(8,128)(2,1)S(1)} %copy.103), channel_id=1, replica_groups=mesh['grp'=2,'ep'=64,'tp'=2] {'tp'}, dimensions={0} | all-to-all | bytes 4194304 | tf_op jit(solution)/shard_map/all_to_all | solution.py:45
  130.7 2.2 %reduce_sum.94 = bf16[64,2,4,1024]{3,0,2,1:T(8,128)(2,1)S(1)} reduce(bf16[2,64,1,2,4,1024]{5,1,4,3,2,0:T(8,128)(2,1)} %all_to_all.22, bf16[]{:T(256)} %constant.37.clone.1), dimensions={0,2}, to_apply=%region_9.10 | reduce | flops 524288 | bytes 3145730 | tf_op jit(solution)/shard_map/reduce_sum | solution.py:46
  133.0 1.8 copy.105
  134.8 7.6 %all-to-all-start.3 = ((bf16[64,2,4,1024]{3,2,1,0:T(4,128)(2,1)}), bf16[64,2,4,1024]{3,2,1,0:T(4,128)(2,1)S(1)}, u32[]{:S(2)}, u32[]{:S(2)}) async-start(bf16[64,2,4,1024]{3,2,1,0:T(4,128)(2,1)} %copy.105), calls=%async_computation.3 | async-start | bytes 2097152 | tf_op jit(solution)/shard_map/all_to_all | solution.py:188
  142.4 1.4 multiply_reduce_fusion.1
  144.7 1.2 fusion.91
  145.9 1.7 fusion.36
  147.5 49.0 %all-to-all-done.3 = bf16[64,2,4,1024]{3,2,1,0:T(4,128)(2,1)S(1)} async-done(((bf16[64,2,4,1024]{3,2,1,0:T(4,128)(2,1)}), bf16[64,2,4,1024]{3,2,1,0:T(4,128)(2,1)S(1)}, u32[]{:S(2)}, u32[]{:S(2)}) %all-to-all-start.3) | async-done | bytes 1048608 | tf_op jit(solution)/shard_map/all_to_all | solution.py:188
  196.5 1.1 reshape.164
  197.6 2.1 %fusion.34 = bf16[16,1024]{1,0:T(8,128)(2,1)} fusion(f32[16,1024]{1,0:T(8,128)S(1)} %fusion.36, f32[16,1024]{1,0:T(8,128)S(1)} %get-tuple-element.11, bf16[16,512]{1,0:T(8,128)(2,1)S(1)} %select_reduce_fusion.1, bf16[512,1024]{1,0:T(8,128)(2,1)} %reshape.164), kind=kOutput, calls=%fused_computation.31 | convolution fusion | flops 16826368 | bytes 1228800 | tf_op jit(solution)/shard_map/dot_general | solution.py:192
  (59 shorter events, 8.7 us)
Async XLA Ops:
  0.6 22.4 %copy-start = (bf16[1024,1024]{1,0:T(8,128)(2,1)S(1)}, bf16[1024,1024]{1,0:T(8,128)(2,1)}, u32[]{:S(2)}) copy-start(bf16[1024,1024]{1,0:T(8,128)(2,1)} %param.40) | copy-start | bytes 6291460
  0.6 7.6 %copy-start.3 = (bf16[256,1024]{1,0:T(8,128)(2,1)S(1)}, bf16[256,1024]{1,0:T(8,128)(2,1)}, u32[]{:S(2)}) copy-start(bf16[256,1024]{1,0:T(8,128)(2,1)} %param.38) | copy-start | bytes 1572868
  16.6 6.5 %copy-start.2 = (bf16[16,1024]{1,0:T(8,128)(2,1)S(1)}, bf16[16,1024]{1,0:T(8,128)(2,1)}, u32[]{:S(2)}) copy-start(bf16[16,1024]{1,0:T(8,128)(2,1)} %param.24) | copy-start | bytes 98308
  21.3 2.2 %copy-start.5 = (s32[16,4]{0,1:T(4,128)S(1)}, s32[16,4]{0,1:T(4,128)}, u32[]{:S(2)}) copy-start(s32[16,4]{0,1:T(4,128)} %param.28) | copy-start | bytes 772
  21.4 3.0 %copy-start.6 = (f32[1024]{0:T(1024)S(1)}, f32[1024]{0:T(1024)}, u32[]{:S(2)}) copy-start(f32[1024]{0:T(1024)} %param.41) | copy-start | bytes 12292
  110.0 6.9 %copy-start.9 = (bf16[2,1024,128]{2,1,0:T(8,128)(2,1)S(1)}, bf16[2,1024,128]{2,1,0:T(8,128)(2,1)}, u32[]{:S(2)}) copy-start(bf16[2,1024,128]{2,1,0:T(8,128)(2,1)} %param.42) | copy-start | bytes 1572868
  115.5 1.4 copy-start.1
  116.9 1.5 copy-start.10
  116.9 1.5 copy-start.11
  132.9 9.5 %copy-start.4 = (f32[1024]{0:T(1024)S(1)}, f32[1024]{0:T(1024)}, u32[]{:S(2)}) copy-start(f32[1024]{0:T(1024)} %param.30) | copy-start | bytes 12292
  133.0 10.8 %copy-start.8 = (f32[256]{0:T(256)S(1)}, f32[256]{0:T(256)}, u32[]{:S(2)}) copy-start(f32[256]{0:T(256)} %param.34) | copy-start | bytes 3076
  133.0 11.6 %copy-start.7 = (f32[16,4]{0,1:T(4,128)S(1)}, f32[16,4]{0,1:T(4,128)}, u32[]{:S(2)}) copy-start(f32[16,4]{0,1:T(4,128)} %param.29) | copy-start | bytes 772
  134.8 61.7 %all-to-all-start.3 = ((bf16[64,2,4,1024]{3,2,1,0:T(4,128)(2,1)}), bf16[64,2,4,1024]{3,2,1,0:T(4,128)(2,1)S(1)}, u32[]{:S(2)}, u32[]{:S(2)}) async-start(bf16[64,2,4,1024]{3,2,1,0:T(4,128)(2,1)} %copy.105), calls=%async_computation.3 | async-start | bytes 2097152 | tf_op jit(solution)/shard_map/all_to_all | solution.py:188
where the time goes:
time: 201 us; the launch traced here: 200 us
  blocking collectives  94.8 us (47%)
  waiting for transfers between devices  49 us (24%)
  matrix products  30.3 us (15%)
  local copies, waits for them, and re-layouts  10.3 us (5%)
  starting transfers between devices  7.61 us (4%)
  other arithmetic  6.69 us (3%)
    all_to_all x1, blocking collectives, local(): lax.all_to_all(outbox, 'ep', split_axis=0, concat_axis=0, tiled=True)  82.9 us
    all_to_all x1, waiting for transfers between devices, local(): lax.all_to_all(summed[:, 0].astype(jnp.bfloat16), 'ep', split_axis=0, con...  49 us
    all_to_all x1, starting transfers between devices, local(): lax.all_to_all(summed[:, 0].astype(jnp.bfloat16), 'ep', split_axis=0, con...  7.61 us
    all_to_all x1, blocking collectives, sent_and_summed(): blocks = lax.all_to_all(split_up(value, dim, count), axis, 0, 0, tiled=True)  6.33 us
    dot_general x1, matrix products, local(): jnp.einsum('shc,stc->sht', query_latent, latent_cache, preferred_element_...  5.67 us
    all_to_all x1, blocking collectives, copy_for_each(): lax.all_to_all(jnp.broadcast_to(value[None], (count, *value.shape)), axis...  5.57 us
    dot_general x1, matrix products, local(): jnp.einsum('sht,stc->shc', weights.astype(jnp.bfloat16), latent_cache, pr...  4.74 us
    dot_general x1, matrix products, local(): jnp.einsum('aterf,efd->aterd', hidden, w_expert_down, preferred_element_t...  4.22 us
  transfers between devices with their start and end apart: 1, of which 1 were waited for; matrix products, arithmetic and copies ran while one was open for 3% of the time, Pallas kernels for 0%

commit v1 on v0

--- a/solution.py
+++ b/solution.py
@@ -1,6 +1,10 @@
+import functools
+
 import jax
 import jax.numpy as jnp
 from jax import lax
+from jax.experimental import pallas as pl
+from jax.experimental.pallas import tpu as pltpu
 from jax.sharding import PartitionSpec as P
 
 D = 1024
@@ -9,41 +13,11 @@
 NOPE = 64
 ROPE = 32
 VDIM = 64
-CAP = 4
 
 
 norm_eps = 1e-06
 rope_theta = 10000.0
 masked_score = -1e30
-
-
-def copy_for_each(value, axis):
-    count = lax.axis_size(axis)
-    return lax.all_to_all(
-        jnp.broadcast_to(value[None], (count, *value.shape)), axis, 0, 0, tiled=True
-    )
-
-
-def joined_along(blocks, dim):
-    blocks = jnp.moveaxis(blocks, 0, dim)
-    dims = blocks.shape
-    return blocks.reshape(*dims[:dim], dims[dim] * dims[dim + 1], *dims[dim + 2 :])
-
-
-def gathered_copies(value, axis, dim):
-    blocks = copy_for_each(value, axis)
-    return joined_along(blocks, dim)
-
-
-def split_up(value, dim, count):
-    before, after = (value.shape[:dim], value.shape[dim + 1 :])
-    return jnp.moveaxis(value.reshape(*before, count, -1, *after), dim, 0)
-
-
-def sent_and_summed(value, axis, dim):
-    count = lax.axis_size(axis)
-    blocks = lax.all_to_all(split_up(value, dim, count), axis, 0, 0, tiled=True)
-    return jnp.sum(blocks.astype(jnp.float32), axis=0)
 
 
 def rms_scale(values, gain_vec):
@@ -69,13 +43,449 @@
     )
 
 
-def slot_numbers(expert_ids, expert_count):
-    flat_ids = expert_ids.reshape(-1)
-    onehot = (flat_ids[:, None] == jnp.arange(expert_count, dtype=jnp.int32)[None, :]).astype(
-        jnp.int32
-    )
-    rank_before = jnp.cumsum(onehot, axis=0) - onehot
-    return jnp.sum(rank_before * onehot, axis=1).reshape(expert_ids.shape)
+MESH = pl.DeviceIdType.MESH
+RING_X = 4
+EFF2 = 256
+HALF = 128
+
+
+def remote(src, dst, send_sem, recv_sem, **where):
+    return pltpu.make_async_remote_copy(
+        src_ref=src,
+        dst_ref=dst,
+        send_sem=send_sem,
+        recv_sem=recv_sem,
+        device_id=where,
+        device_id_type=MESH,
+    )
+
+
+def moe_kernel(
+    ep_size,
+    x_ref,
+    meta_ref,
+    base_ref,
+    gate_hbm,
+    up_hbm,
+    down_hbm,
+    out_ref,
+    rows_buf,
+    part_buf,
+    meta_buf,
+    w_in,
+    w_down,
+    half_l,
+    half_r,
+    full_l,
+    full_r,
+    chain_a,
+    chain_b,
+    w_local,
+    w_send,
+    w_recv,
+    m_send,
+    m_recv,
+    zs,
+    zr,
+    xs,
+    xr,
+    rs_xs,
+    rs_xr,
+    rs_zs,
+    rs_zr,
+):
+    ring_z = ep_size // RING_X
+    far = ring_z // 2
+    me = lax.axis_index("ep")
+    core = lax.axis_index("tp")
+    z = me // RING_X
+    x = me % RING_X
+    low, high = pl.ds(0, D // 2), pl.ds(D // 2, D // 2)
+
+    def at(zz, xx):
+        return lax.rem(zz + 2 * ring_z, ring_z) * RING_X + lax.rem(xx + 2 * RING_X, RING_X)
+
+    right, left = at(z, x + 1), at(z, x - 1)
+    above, below = at(z + 1, x), at(z - 1, x)
+
+    barrier = pltpu.get_barrier_semaphore()
+
+    def greet(step, carry):
+        pl.semaphore_signal(
+            barrier, inc=1, device_id={"ep": lax.rem(me + step, ep_size)}, device_id_type=MESH
+        )
+        return carry
+
+    lax.fori_loop(1, ep_size, greet, 0)
+    pl.semaphore_signal(barrier, inc=1, device_id={"tp": 1 - core}, device_id_type=MESH)
+
+    pieces = []
+    for e in range(2):
+        for kind, hbm in enumerate((gate_hbm, up_hbm)):
+            col = pl.multiple_of((e * 2 + kind) * EFF2 + core * HALF, HALF)
+            pieces.append((hbm.at[e], w_in.at[:, pl.ds(col, HALF)]))
+        row = pl.multiple_of(e * EFF2 + core * HALF, HALF)
+        pieces.append((down_hbm.at[e], w_down.at[pl.ds(row, HALF), :]))
+    local_copies = [
+        pltpu.make_async_copy(s, d, w_local.at[i]) for i, (s, d) in enumerate(pieces)
+    ]
+    for copy in local_copies:
+        copy.start()
+    rows_buf[me] = x_ref[...]
+    meta_buf[me] = meta_ref[...]
+
+    pl.semaphore_wait(barrier, ep_size)
+
+    def z_up(t):
+        slot = at(z - t, x)
+        return remote(
+            x_ref if isinstance(t, int) and t == 0 else rows_buf.at[slot],
+            rows_buf.at[slot], zs.at[0, t], zr.at[0, t], ep=above,
+        )
+
+    def z_down(t):
+        slot = at(z + t, x)
+        return remote(
+            x_ref if isinstance(t, int) and t == 0 else rows_buf.at[slot],
+            rows_buf.at[slot], zs.at[1, t], zr.at[1, t], ep=below,
+        )
+
+    def x_near(p, zz):
+        slot = at(zz, x)
+        src = x_ref if isinstance(p, int) and p == 0 else rows_buf.at[slot]
+        return (
+            remote(src, rows_buf.at[slot], xs.at[0, p], xr.at[0, p], ep=right),
+            remote(src, rows_buf.at[slot], xs.at[1, p], xr.at[1, p], ep=left),
+        )
+
+    def x_far(p, zz):
+        from_left, from_right = at(zz, x - 1), at(zz, x + 1)
+        return (
+            remote(
+                rows_buf.at[from_left, :, low], rows_buf.at[from_left, :, low],
+                xs.at[2, p], xr.at[2, p], ep=right,
+            ),
+            remote(
+                rows_buf.at[from_right, :, high], rows_buf.at[from_right, :, high],
+                xs.at[3, p], xr.at[3, p], ep=left,
+            ),
+        )
+
+    def start(copies):
+        for copy in copies:
+            copy.start()
+
+    def arrived(copies):
+        for copy in copies:
+            copy.wait_recv()
+
+    def sent(copies):
+        for copy in copies:
+            copy.wait_send()
+
+    z_up(0).start()
+    z_down(0).start()
+    start(x_near(0, z))
+
+    def meta_copy(step):
+        return remote(
+            meta_ref, meta_buf.at[me], m_send, m_recv, ep=lax.rem(me + step, ep_size)
+        )
+
+    def meta_go(step, carry):
+        meta_copy(step).start()
+        return carry
+
+    lax.fori_loop(1, ep_size, meta_go, 0)
+
+    remote_copies = [
+        remote(s, d, w_send.at[i], w_recv.at[i], tp=1 - core) for i, (s, d) in enumerate(pieces)
+    ]
+    start(remote_copies)
+
+    lane = lax.broadcasted_iota(jnp.int32, (16, 128), 1)
+    row = lax.broadcasted_iota(jnp.int32, (16, 128), 0)
+    pick = (lane < 64) & (lane % 16 == row)
+    first_expert = (2 * me).astype(jnp.float32)
+
+    def weight_columns(slot):
+        ids = meta_buf[slot]
+        scale = pltpu.roll(ids, 64, 1)
+        columns = []
+        for e in range(2):
+            chosen = jnp.where(ids == first_expert + e, scale, 0.0)
+            chosen = jnp.where(pick, jnp.broadcast_to(chosen, (16, 128)), 0.0)
+            columns.append(jnp.sum(chosen, axis=1, keepdims=True))
+        return columns
+
+    def experts(plane_a, plane_b):
+        planes = [lax.rem(plane + 2 * ring_z, ring_z) for plane in (plane_a, plane_b)]
+        rows = jnp.concatenate(
+            [rows_buf[pl.ds(plane * RING_X, RING_X)].reshape(RING_X * 16, D) for plane in planes], 0
+        )
+        scales = [weight_columns(plane * RING_X + k) for plane in planes for k in range(RING_X)]
+        hidden = []
+        for e in range(2):
+            gates = jnp.dot(
+                rows, w_in[:, 2 * e * EFF2 : (2 * e + 1) * EFF2], preferred_element_type=jnp.float32
+            )
+            ups = jnp.dot(
+                rows, w_in[:, (2 * e + 1) * EFF2 : (2 * e + 2) * EFF2],
+                preferred_element_type=jnp.float32,
+            )
+            scale = jnp.concatenate([s[e] for s in scales], axis=0)
+            hidden.append((gates / (1.0 + jnp.exp(-gates)) * ups * scale).astype(jnp.bfloat16))
+        total = jnp.dot(
+            jnp.concatenate(hidden, axis=1), w_down[...], preferred_element_type=jnp.float32
+        ).astype(jnp.bfloat16)
+        for k, plane in enumerate(planes):
+            part_buf[pl.ds(plane * RING_X, RING_X)] = total[
+                k * RING_X * 16 : (k + 1) * RING_X * 16
+            ].reshape(RING_X, 16, D)
+
+    def far_of(t):
+        return x_far(2 * t + 1, z - 1 - t) + x_far(2 * t + 2, z + 1 + t)
+
+    def near_of(t):
+        return x_near(2 * t + 1, z - 1 - t) + x_near(2 * t + 2, z + 1 + t)
+
+    z_up(0).wait_recv()
+    z_up(1).start()
+    z_down(0).wait_recv()
+    z_down(1).start()
+    start(near_of(0))
+    arrived(x_near(0, z))
+    start(x_far(0, z))
+
+    for copy in local_copies:
+        copy.wait()
+    for copy in remote_copies:
+        copy.wait()
+    whole_meta = meta_buf.at[pl.ds(0, ep_size - 1)]
+    pltpu.make_async_copy(whole_meta, whole_meta, m_recv).wait()
+    pltpu.make_async_copy(whole_meta, whole_meta, m_send).wait()
+
+    z_up(1).wait_recv()
+    z_up(2).start()
+    z_down(1).wait_recv()
+    z_down(2).start()
+    start(near_of(1))
+    arrived(near_of(0))
+    start(far_of(0))
+    arrived(x_far(0, z))
+
+    def gather_step(t, carry):
+        z_up(t).wait_recv()
+        z_up(t + 1).start()
+        z_down(t).wait_recv()
+
+        @pl.when(t < far - 2)
+        def _():
+            z_down(t + 1).start()
+
+        start(near_of(t))
+        arrived(near_of(t - 1))
+        start(far_of(t - 1))
+        arrived(far_of(t - 2))
+        experts(z - (t - 1), z + (t - 1))
+        return carry
+
+    lax.fori_loop(2, far - 1, gather_step, 0)
+    last = far - 1
+    z_up(last).wait_recv()
+    start(x_near(2 * last + 1, z - far))
+    arrived(near_of(last - 1))
+    start(far_of(last - 1))
+    arrived(far_of(last - 2))
+    experts(z - last + 1, z + last - 1)
+    arrived(x_near(2 * last + 1, z - far))
+    start(x_far(2 * last + 1, z - far))
+    arrived(far_of(last - 1))
+    experts(z - last, z + last)
+    arrived(x_far(2 * last + 1, z - far))
+    experts(z, z - far)
+
+    def plane_of(i, side):
+        return z - (far - i) if side == 0 else z + (far - 1 - i)
+
+    def x1(i):
+        copies = []
+        for side in range(2):
+            zz, p = plane_of(i, side), 2 * i + side
+            opposite = at(zz, x + 2)
+            copies.append(
+                remote(
+                    part_buf.at[opposite, :, low], half_l.at[p],
+                    rs_xs.at[0, p], rs_xr.at[0, p], ep=right,
+                )
+            )
+            copies.append(
+                remote(
+                    part_buf.at[opposite, :, high], half_r.at[p],
+                    rs_xs.at[1, p], rs_xr.at[1, p], ep=left,
+                )
+            )
+        return copies
+
+    def x2(i):
+        copies = []
+        for side in range(2):
+            zz, p = plane_of(i, side), 2 * i + side
+            copies.append(
+                remote(
+                    part_buf.at[at(zz, x + 1)], full_l.at[p],
+                    rs_xs.at[2, p], rs_xr.at[2, p], ep=right,
+                )
+            )
+            copies.append(
+                remote(
+                    part_buf.at[at(zz, x - 1)], full_r.at[p],
+                    rs_xs.at[3, p], rs_xr.at[3, p], ep=left,
+                )
+            )
+        return copies
+
+    def x2_add(i):
+        for side in range(2):
+            zz, p = plane_of(i, side), 2 * i + side
+            to_right, to_left = at(zz, x + 1), at(zz, x - 1)
+            part_buf[to_right, :, low] = part_buf[to_right, :, low] + half_l[p]
+            part_buf[to_left, :, high] = part_buf[to_left, :, high] + half_r[p]
+
+    def chain(i, side):
+        slot = at(plane_of(i, side), x)
+        buf = chain_a if side == 0 else chain_b
+        return remote(
+            part_buf.at[slot], buf.at[i], rs_zs.at[side, i], rs_zr.at[side, i],
+            ep=below if side == 0 else above,
+        )
+
+    def own_sum(i, side):
+        slot, p = at(plane_of(i, side), x), 2 * i + side
+        return (
+            part_buf[slot].astype(jnp.float32)
+            + full_l[p].astype(jnp.float32)
+            + full_r[p].astype(jnp.float32)
+        )
+
+    def store(i, side, total):
+        part_buf[at(plane_of(i, side), x)] = total.astype(jnp.bfloat16)
+
+    start(x1(0))
+    start(x1(1))
+    arrived(x1(0))
+    x2_add(0)
+    start(x2(0))
+    arrived(x2(0))
+    for side in range(2):
+        store(0, side, own_sum(0, side))
+        chain(0, side).start()
+    arrived(x1(1))
+    x2_add(1)
+    start(x2(1))
+    start(x1(2))
+
+    def sum_step(i, carry):
+        arrived(x2(i))
+        for side in range(2):
+            total = own_sum(i, side)
+            chain(i - 1, side).wait_recv()
+            buf = chain_a if side == 0 else chain_b
+            store(i, side, total + buf[i - 1].astype(jnp.float32))
+            chain(i, side).start()
+        arrived(x1(i + 1))
+        x2_add(i + 1)
+        start(x2(i + 1))
+
+        @pl.when(i < far - 2)
+        def _():
+            start(x1(i + 2))
+
+        return carry
+
+    lax.fori_loop(1, far - 1, sum_step, 0)
+    arrived(x2(last))
+    total = own_sum(last, 0)
+    chain(last - 1, 0).wait_recv()
+    store(last, 0, total + chain_a[last - 1].astype(jnp.float32))
+    chain(last, 0).start()
+    total = own_sum(last, 1) + base_ref[...]
+    chain(last - 1, 1).wait_recv()
+    total = total + chain_b[last - 1].astype(jnp.float32)
+    chain(last, 0).wait_recv()
+    out_ref[...] = (total + chain_a[last].astype(jnp.float32)).astype(jnp.bfloat16)
+
+    def drain_z(t, carry):
+        z_up(t).wait_send()
+        chain(t, 0).wait_send()
+
+        @pl.when(t < far - 1)
+        def _():
+            z_down(t).wait_send()
+            chain(t, 1).wait_send()
+
+        sent(x1(t))
+        sent(x2(t))
+        return carry
+
+    lax.fori_loop(0, far, drain_z, 0)
+
+    def drain_x(p, carry):
+        zz = z
+        sent(x_near(p, zz))
+        sent(x_far(p, zz))
+        return carry
+
+    lax.fori_loop(0, 2 * far, drain_x, 0)
+
+
+def moe(rows, meta, base, w_gate, w_up, w_down):
+    ep_size = lax.axis_size("ep")
+    ring_z = ep_size // RING_X
+    far = ring_z // 2
+    count = rows.shape[0]
+    bf = jnp.bfloat16
+    dma = pltpu.SemaphoreType.DMA
+    vm = pl.BlockSpec(memory_space=pltpu.VMEM)
+    anywhere = pl.BlockSpec(memory_space=pl.ANY)
+    block = (count, D)
+    half = (count, D // 2)
+    return pl.pallas_call(
+        functools.partial(moe_kernel, ep_size),
+        out_shape=jax.ShapeDtypeStruct((count, D), bf),
+        in_specs=[vm, vm, vm, anywhere, anywhere, anywhere],
+        out_specs=vm,
+        scratch_shapes=[
+            pltpu.VMEM((ep_size, *block), bf),
+            pltpu.VMEM((ep_size, *block), bf),
+            pltpu.VMEM((ep_size, 1, 128), jnp.float32),
+            pltpu.VMEM((D, 4 * EFF2), bf),
+            pltpu.VMEM((2 * EFF2, D), bf),
+            pltpu.VMEM((ring_z, *half), bf),
+            pltpu.VMEM((ring_z, *half), bf),
+            pltpu.VMEM((ring_z, *block), bf),
+            pltpu.VMEM((ring_z, *block), bf),
+            pltpu.VMEM((far, *block), bf),
+            pltpu.VMEM((far, *block), bf),
+            dma((6,)),
+            dma((6,)),
+            dma((6,)),
+            dma,
+            dma,
+            dma((2, far)),
+            dma((2, far)),
+            dma((4, ring_z)),
+            dma((4, ring_z)),
+            dma((4, ring_z)),
+            dma((4, ring_z)),
+            dma((2, far)),
+            dma((2, far)),
+        ],
+        compiler_params=pltpu.CompilerParams(
+            collective_id=0, has_side_effects=True, vmem_limit_bytes=40 * 1024 * 1024
+        ),
+        name="moe",
+    )(rows, meta, base, w_gate, w_up, w_down)
 
 
 def local(
@@ -162,35 +572,11 @@
     shared_up = jnp.dot(normed_ffn, w_shared_up, preferred_element_type=jnp.float32)
     shared_hidden = (jax.nn.silu(shared_gate) * shared_up).astype(jnp.bfloat16)
     shared_out = jnp.dot(shared_hidden, w_shared_down, preferred_element_type=jnp.float32)
-    ep_size = lax.axis_size("ep")
-    local_experts = w_expert_gate.shape[0]
-    expert_count = local_experts * ep_size
-    slot_count = expert_count * CAP
-    slots = slot_numbers(expert_ids, expert_count)
-    target = expert_ids * CAP + slots
-    slot_match = target[:, :, None] == jnp.arange(slot_count, dtype=jnp.int32)[None, None, :]
-    spread = jnp.sum(slot_match.astype(jnp.bfloat16), axis=1)
-    outbox = jnp.einsum("sn,sd->nd", spread, normed_ffn, preferred_element_type=jnp.float32)
-    outbox = outbox.astype(jnp.bfloat16).reshape(ep_size, local_experts, CAP, D)
-    landed = lax.all_to_all(outbox, "ep", split_axis=0, concat_axis=0, tiled=True)
-    arrived = gathered_copies(landed[:, None], "tp", 1)
-    gate_value = jnp.einsum(
-        "aterd,edf->aterf", arrived, w_expert_gate, preferred_element_type=jnp.float32
-    )
-    up_value = jnp.einsum(
-        "aterd,edf->aterf", arrived, w_expert_up, preferred_element_type=jnp.float32
-    )
-    hidden = (jax.nn.silu(gate_value) * up_value).astype(jnp.bfloat16)
-    partial_value = jnp.einsum(
-        "aterf,efd->aterd", hidden, w_expert_down, preferred_element_type=jnp.float32
-    )
-    summed = sent_and_summed(partial_value.astype(jnp.bfloat16), "tp", 1)
-    returned = lax.all_to_all(
-        summed[:, 0].astype(jnp.bfloat16), "ep", split_axis=0, concat_axis=0, tiled=True
-    )
-    slot_weights = jnp.sum(jnp.where(slot_match, route_weights[:, :, None], 0.0), axis=1)
-    routed = jnp.dot(slot_weights, returned.reshape(slot_count, D).astype(jnp.float32))
-    mixed_out = (hidden_state.astype(jnp.float32) + routed + shared_out).astype(jnp.bfloat16)
+    meta = jnp.concatenate(
+        [expert_ids.T.astype(jnp.float32).reshape(1, -1), route_weights.T.reshape(1, -1)], axis=1
+    )
+    base = hidden_state.astype(jnp.float32) + shared_out
+    mixed_out = moe(normed_ffn, meta, base, w_expert_gate, w_expert_up, w_expert_down)
     return (mixed_out, new_entry)
 
 

time: 201 us -> 148 us (0.74)
  Pallas kernels: 0 us -> 111 us
  blocking collectives: 94.8 us -> 0 us
  waiting for transfers between devices: 49 us -> 0 us
  starting transfers between devices: 7.61 us -> 0 us
  matrix products: 30.3 us -> 24.8 us
  other arithmetic: 6.69 us -> 3.35 us
  local copies, waits for them, and re-layouts: 10.3 us -> 7.22 us
    pallas_call x0 -> x1, Pallas kernels: none -> 111 us  [moe(): pl.pallas_call(functools.partial(moe_kernel, ep_size), out_shape=jax.Shap...]
    all_to_all x3 -> x0, blocking collectives: 94.8 us -> none  [the longest x1 82.9 us: local(): lax.all_to_all(outbox, 'ep', split_axis=0, concat_axis=0, tiled=True)]
    all_to_all x1 -> x0, waiting for transfers between devices: 49 us -> none  [local(): lax.all_to_all(summed[:, 0].astype(jnp.bfloat16), 'ep', split_axis=0, con...]
    dot_general x4 -> x0, matrix products: 8.27 us -> none  [the longest x1 4.22 us: local(): jnp.einsum('aterf,efd->aterd', hidden, w_expert_down, preferred_element_t...]
    all_to_all x1 -> x0, starting transfers between devices: 7.61 us -> none  [local(): lax.all_to_all(summed[:, 0].astype(jnp.bfloat16), 'ep', split_axis=0, con...]
    unnamed x27, local copies, waits for them, and re-layouts: 2.97 us -> 6.69 us
    reduce_sum x4 -> x0, other arithmetic: 2.58 us -> none  [the longest x1 2.22 us: sent_and_summed(): return jnp.sum(blocks.astype(jnp.float32), axis=0)]
    reshape x4 -> x2, local copies, waits for them, and re-layouts: 2.51 us -> 0.16 us  [the longest x1 0.08 us: local(): expert_ids.T.astype(jnp.float32).reshape(1, -1)]
  transfers between devices with their start and end apart: 1 -> 0, of which waited for: 1 -> 0; matrix products, arithmetic and copies ran while one was open for 3% -> 0% of each run, Pallas kernels for 0% -> 0%
where the time goes in v1:
time: 148 us; the launch traced here: 147 us
  Pallas kernels  111 us (75%)
  matrix products  24.8 us (17%)
  local copies, waits for them, and re-layouts  7.22 us (5%)
  other arithmetic  3.35 us (2%)
    pallas_call x1, Pallas kernels, moe(): pl.pallas_call(functools.partial(moe_kernel, ep_size), out_shape=jax.Shap...  111 us
    unnamed x27, local copies, waits for them, and re-layouts  6.69 us
    dot_general x1, matrix products, local(): jnp.einsum('shc,stc->sht', query_latent, latent_cache, preferred_element_...  5.67 us
    dot_general x1, matrix products, local(): jnp.einsum('sht,stc->shc', weights.astype(jnp.bfloat16), latent_cache, pr...  5.41 us

profile of v1, /device:TPU:40, one launch (start us, length us, event | category | flops | bytes accessed | tf_op | source)
XLA Modules:
  0.0 147.0 jit_solution(1927046770685868364)
XLA Ops:
  0.6 1.0 fusion.21
  1.7 1.4 multiply_reduce_fusion.2
  3.1 1.2 fusion.46
  4.4 1.1 fusion.47
  5.5 0.7 convert_element_type.65
  6.1 0.1 subtract_convert_fusion.1
  6.4 1.6 %fusion.24 = f32[16,16,1024]{2,1,0:T(8,128)S(1)} fusion(bf16[16,1024,32]{1,2,0:T(8,128)(2,1)} %param.26, bf16[16,16,16]{2,1,0:T(8,128)(2,1)S(1)} %get-tuple-element.3, bf16[16,16,16]{2,1,0:T(8,128)(2,1)S(1)} %get-tuple-element.2), kind=kOutput, calls=%fused_computation.33 | convolution fusion | flops 16809984 | bytes 2113536 | tf_op jit(solution)/shard_map/shr,str->sht/dot_general | solution.py:545
  8.0 1.3 convolution_convert_fusion.2
  9.4 2.0 %copy.30 = bf16[256,1024]{0,1:T(8,128)(2,1)} copy(bf16[256,1024]{1,0:T(8,128)(2,1)} %param.38) | data formatting | bytes 1048576 | tf_op args[14]
  11.4 1.2 fusion.11
  12.6 5.7 %fusion.9 = f32[16,16,1024]{2,1,0:T(8,128)S(1)} fusion(f32[16,16,1024]{2,1,0:T(8,128)S(1)} %fusion.24, bf16[16,1024,256]{2,1,0:T(8,128)(2,1)} %param.25, bf16[16,16,256]{2,0,1:T(8,128)(2,1)S(1)} %fusion.11), kind=kOutput, calls=%fused_computation.7 | convolution fusion | flops 134742016 | bytes 10616832 | tf_op jit(solution)/shard_map/shc,stc->sht/dot_general | solution.py:544
  18.4 0.9 copy-done.4
  19.3 0.4 fusion.53
  19.7 5.4 %fusion.10 = bf16[16,16,256]{2,1,0:T(8,128)(2,1)S(1)} fusion(bf16[16,1024,256]{2,1,0:T(8,128)(2,1)} %param.25, f32[16,16]{1,0:T(8,128)S(1)} %fusion.53, f32[16,16,1024]{2,1,0:T(8,128)} %copy-done.4, pred[16,1024]{1,0:T(8,128)(4,1)S(1)} %iota_compare_fusion), kind=kOutput, calls=%fused_computation.10 | convolution fusion | flops 135398656 | bytes 9585664 | tf_op jit(solution)/shard_map/sht,stc->shc/dot_general | solution.py:553
  25.2 2.0 %copy.33 = bf16[256,1024]{0,1:T(8,128)(2,1)} copy(bf16[256,1024]{1,0:T(8,128)(2,1)} %param.39) | data formatting | bytes 1048576 | tf_op args[15]
  27.2 1.3 fusion.12
  28.7 0.5 multiply_reduce_fusion
  29.3 1.2 fusion.54
  30.5 1.7 %convolution_add_fusion.2.base_ref = f32[16,1024]{1,0:T(8,128)S(1)} fusion(f32[16,1024]{1,0:T(8,128)S(1)} %get-tuple-element.11, bf16[256,1024]{1,0:T(8,128)(2,1)} %param.47, bf16[16,1024]{1,0:T(8,128)(2,1)S(1)} %multiply_convert_fusion.x_ref, bf16[1024,256]{1,0:T(8,128)(2,1)} %param.46, f32[16,256]{1,0:T(8,128)S(1)} %fusion.54), kind=kOutput, calls=%fused_computation.15 | convolution fusion | flops 16818176 | bytes 1228800 | tf_op jit(solution)/shard_map/dot_general | solution.py:574
  32.4 1.0 copy-done.3
  33.5 110.7 %moe.1 = bf16[16,1024]{1,0:T(8,128)(2,1)S(1)} custom-call(bf16[16,1024]{1,0:T(8,128)(2,1)S(1)} %multiply_convert_fusion.x_ref, f32[1,128]{1,0:T(1,128)S(1)} %pad_maximum_fusion.1.meta_ref, f32[16,1024]{1,0:T(8,128)S(1)} %convolution_add_fusion.2.base_ref, bf16[2,1024,128]{2,1,0:T(8,128)(2,1)S(1)} %copy-done.1, bf16[2,1024,128]{2,1,0:T(8,128)(2,1)S(1)} %copy-done.2, ...), custom_call_target="tpu_custom_call" | custom-call | tf_op jit(solution)/shard_map/moe/pallas_call | solution.py:453
  144.2 1.4 multiply_reduce_fusion.1
  145.7 0.7 pad_maximum_fusion
  146.4 0.6 copy.43
  (39 shorter events, 1.1 us)
Async XLA Ops:
  0.6 28.0 %copy-start = (bf16[1024,1024]{1,0:T(8,128)(2,1)S(1)}, bf16[1024,1024]{1,0:T(8,128)(2,1)}, u32[]{:S(2)}) copy-start(bf16[1024,1024]{1,0:T(8,128)(2,1)} %param.40) | copy-start | bytes 6291460
  1.7 16.6 %copy-start.11 = (s32[16]{0:T(128)S(1)}, s32[16]{0:T(128)}, u32[]{:S(2)}) copy-start(s32[16]{0:T(128)} %param.27) | copy-start | bytes 196
  18.3 1.0 copy-start.4
  18.3 10.3 %copy-start.5 = (bf16[16,1024]{1,0:T(8,128)(2,1)S(1)}, bf16[16,1024]{1,0:T(8,128)(2,1)}, u32[]{:S(2)}) copy-start(bf16[16,1024]{1,0:T(8,128)(2,1)} %param.24) | copy-start | bytes 98308
  18.3 10.8 %copy-start.7 = (f32[1024]{0:T(1024)S(1)}, f32[1024]{0:T(1024)}, u32[]{:S(2)}) copy-start(f32[1024]{0:T(1024)} %param.41) | copy-start | bytes 12292
  19.3 12.8 %copy-start.9 = (s32[16,4]{0,1:T(4,128)S(1)}, s32[16,4]{0,1:T(4,128)}, u32[]{:S(2)}) copy-start(s32[16,4]{0,1:T(4,128)} %param.28) | copy-start | bytes 772
  19.3 12.9 %copy-start.8 = (f32[16,4]{0,1:T(4,128)S(1)}, f32[16,4]{0,1:T(4,128)}, u32[]{:S(2)}) copy-start(f32[16,4]{0,1:T(4,128)} %param.29) | copy-start | bytes 772
  19.3 13.1 %copy-start.1 = (bf16[2,1024,128]{2,1,0:T(8,128)(2,1)S(1)}, bf16[2,1024,128]{2,1,0:T(8,128)(2,1)}, u32[]{:S(2)}) copy-start(bf16[2,1024,128]{2,1,0:T(8,128)(2,1)} %gate_hbm.1) | copy-start | bytes 1572868
  19.3 13.1 %copy-start.2 = (bf16[2,1024,128]{2,1,0:T(8,128)(2,1)S(1)}, bf16[2,1024,128]{2,1,0:T(8,128)(2,1)}, u32[]{:S(2)}) copy-start(bf16[2,1024,128]{2,1,0:T(8,128)(2,1)} %up_hbm.1) | copy-start | bytes 1572868
  19.7 124.5 %copy-start.6 = (f32[1024]{0:T(1024)S(1)}, f32[1024]{0:T(1024)}, u32[]{:S(2)}) copy-start(f32[1024]{0:T(1024)} %param.30) | copy-start | bytes 12292
  19.7 125.9 %copy-start.10 = (f32[256]{0:T(256)S(1)}, f32[256]{0:T(256)}, u32[]{:S(2)}) copy-start(f32[256]{0:T(256)} %param.34) | copy-start | bytes 3076
  32.4 1.0 copy-start.3
